TPU v7x, 32 devices: a whole 2x2x4 slice. The times are simulated.
32 devices in a mesh: sp: 16 (over z, y, x), tp: 2 (over core).
Axes of the slice: x: 2, y: 2, z: 4, core: 2. Of those that a mesh axis runs over, the one named last changes fastest.
Arguments:
- pool_input: bfloat16 [4096, 1024], P('sp', 'tp'), may hold values from -6 to 6
- residual: bfloat16 [4096, 2048], P(('sp', 'tp')), may hold values from -6 to 6
- pool_weight: bfloat16 [4, 256, 256], replicated, may hold values from -0.375 to 0.375
- pool_gain: float32 [1024], replicated, may hold values from 0.1 to 1.9
- out_weight: bfloat16 [1024, 2048], replicated, may hold values from -0.1875 to 0.1875
- norm_gain: float32 [2048], replicated, may hold values from 0.1 to 1.9
- routes: int32 [4096, 4], P(('sp', 'tp')), may hold values from 0 to 15, all different within a row; in each aligned block of 128 rows (0 to 127, 128 to 255, ...) at most 64 rows name the same one
- route_scores: float32 [4096, 4], P(('sp', 'tp')), may hold values from -1 to 1
- gate_weight: bfloat16 [16, 2048, 2048], P('sp', None, 'tp'), may hold values from -0.375 to 0.375
- up_weight: bfloat16 [16, 2048, 2048], P('sp', None, 'tp'), may hold values from -0.375 to 0.375
- down_weight: bfloat16 [16, 2048, 2048], P('sp', 'tp'), may hold values from -0.0234375 to 0.0234375
Outputs:
- layer_out: bfloat16 [4096, 2048], P(('sp', 'tp'))
Inputs may be any that keep to these rules, and one draw needn't show every extreme that they name: `routes`: each row names 4 different experts; among the rows of one device no expert is named more than 64 times, a bound that some block reaches.
All inputs are finite; a program needn't handle non-finite values.
Results may differ from a plain program's by a relative error of at most 0.012.
Values may be sent and summed in bfloat16 or wider, within the bound.
A program may use at most 128 MiB of HBM per device.

v0:
```python
import jax
import jax.numpy as jnp
from jax import lax
from jax.sharding import PartitionSpec as P


def from_behind(block, axis, distance):
    devices = range(lax.axis_size(axis))
    route = [(i - distance, i) for i in devices if i - distance in devices]
    return lax.ppermute(block, axis, route)


def expert_half(rows, gate_local, up_local, down_local):
    gate_pre = jnp.dot(rows, gate_local, preferred_element_type=jnp.float32)
    up_pre = jnp.dot(rows, up_local, preferred_element_type=jnp.float32)
    clipped_gate = jnp.minimum(gate_pre, 7.0)
    clipped_up = jnp.clip(up_pre, -7.0, 7.0)
    activated = ((clipped_up + 1.0) * (clipped_gate * jax.nn.sigmoid(1.702 * clipped_gate))).astype(
        jnp.bfloat16
    )
    return jnp.dot(activated, down_local, preferred_element_type=jnp.float32).astype(jnp.bfloat16)


def shards(
    pool_input,
    residual,
    pool_weight,
    pool_gain,
    out_weight,
    norm_gain,
    routes,
    route_scores,
    gate_weight,
    up_weight,
    down_weight,
):
    tokens_here, width_here = pool_input.shape
    cores = lax.axis_size("tp")
    groups_here = pool_weight.shape[0] // cores
    group_dim = pool_weight.shape[1]
    core_index = lax.axis_index("tp")
    first_group = core_index * groups_here
    previous = from_behind(pool_input[tokens_here - 16 :], "sp", 1)
    extended = jnp.concatenate([previous, pool_input], axis=0).astype(jnp.float32)
    channel_group = first_group + jnp.arange(width_here) // group_dim
    windows = jnp.left_shift(jnp.int32(2), channel_group).astype(jnp.float32)
    totals = jnp.zeros((tokens_here, width_here), jnp.float32)
    for offset in range(16):
        keeper = (windows > offset).astype(jnp.float32)
        totals = totals + extended[16 - offset : 16 - offset + tokens_here] * keeper[None, :]
    positions = (lax.axis_index("sp") * tokens_here + jnp.arange(tokens_here)).astype(jnp.float32)
    counts = jnp.minimum(positions[:, None] + 1.0, windows[None, :])
    pooled = (totals / counts - pool_input.astype(jnp.float32)).astype(jnp.bfloat16)
    local_weight = lax.dynamic_slice_in_dim(pool_weight, first_group, groups_here, 0)
    local_gain = lax.dynamic_slice_in_dim(pool_gain, first_group * group_dim, width_here, 0)
    grouped = jnp.einsum(
        "tgc,gce->tge",
        pooled.reshape(tokens_here, groups_here, group_dim),
        local_weight,
        preferred_element_type=jnp.float32,
    )
    mixer_out = (grouped.reshape(tokens_here, width_here) * local_gain[None, :]).astype(
        jnp.bfloat16
    )
    own_rows = lax.dynamic_slice_in_dim(out_weight, core_index * width_here, width_here, 0)
    projected = lax.psum_scatter(
        jnp.dot(mixer_out, own_rows, preferred_element_type=jnp.float32),
        "tp",
        scatter_dimension=0,
        tiled=True,
    )
    middle = (residual.astype(jnp.float32) + projected).astype(jnp.bfloat16)
    middle_wide = middle.astype(jnp.float32)
    normed = (
        middle_wide
        * lax.rsqrt(jnp.mean(middle_wide * middle_wide, axis=1, keepdims=True) + 1e-05)
        * norm_gain[None, :]
    ).astype(jnp.bfloat16)
    weights = jax.nn.softmax(route_scores, axis=-1)
    row_count, top_count = routes.shape
    model_width = normed.shape[1]
    experts_total = gate_weight.shape[0] * lax.axis_size("sp")
    capacity = row_count * top_count * cores // experts_total
    slots_total = experts_total * capacity
    flat_expert = routes.reshape(-1)
    onehot = (flat_expert[:, None] == jnp.arange(experts_total)[None, :]).astype(jnp.int32)
    ranks = jnp.sum((jnp.cumsum(onehot, axis=0) - 1) * onehot, axis=1)
    slot_ids = flat_expert * capacity + ranks
    picker = jnp.any(
        (jnp.arange(slots_total)[:, None] == slot_ids[None, :]).reshape(
            slots_total, row_count, top_count
        ),
        axis=2,
    ).astype(jnp.bfloat16)
    outgoing = (
        jnp.dot(picker, normed, preferred_element_type=jnp.float32)
        .astype(jnp.bfloat16)
        .reshape(experts_total, capacity, model_width)
    )
    gate_local = gate_weight[0]
    up_local = up_weight[0]
    down_local = down_weight[0]
    paired = lax.all_gather(
        lax.all_to_all(outgoing, "sp", split_axis=0, concat_axis=0, tiled=True),
        "tp",
        axis=0,
        tiled=True,
    )
    partial_value = expert_half(
        paired.reshape(-1, model_width), gate_local, up_local, down_local
    ).reshape(paired.shape)
    summed = (
        lax.psum_scatter(partial_value, "tp", scatter_dimension=0, tiled=True)
        .astype(jnp.float32)
        .astype(jnp.bfloat16)
    )
    expert_out = lax.all_to_all(summed, "sp", split_axis=0, concat_axis=0, tiled=True)
    expert_flat = expert_out.reshape(slots_total, model_width)
    route_rows = (
        expert_flat[slot_ids].astype(jnp.float32).reshape(row_count, top_count, model_width)
    )
    mixture = jnp.sum(route_rows * weights[:, :, None], axis=1)
    return (middle_wide + mixture).astype(jnp.bfloat16)


def solution(mesh):
    return jax.shard_map(
        shards,
        mesh=mesh,
        in_specs=(
            P("sp", "tp"),
            P(("sp", "tp"), None),
            P(),
            P(),
            P(),
            P(),
            P(("sp", "tp"), None),
            P(("sp", "tp"), None),
            P("sp", None, "tp"),
            P("sp", None, "tp"),
            P("sp", "tp", None),
        ),
        out_specs=P(("sp", "tp"), None),
        check_vma=False,
    )
```

profile of v0, /device:TPU:14, one launch (start us, length us, event | category | flops | bytes accessed | tf_op | source)
XLA Modules:
  0.0 336.7 jit_solution(9305086084491702493)
XLA Ops:
  6.5 0.8 slice.57
  7.3 3.4 %collective-permute-start = (bf16[16,512]{1,0:T(8,128)(2,1)S(1)}, bf16[16,512]{1,0:T(8,128)(2,1)S(1)}, u32[]{:S(2)}, u32[]{:S(2)}) collective-permute-start(bf16[16,512]{1,0:T(8,128)(2,1)S(1)} %slice.57), channel_id=1, source_target_pairs={{0,2},{2,4},{4,6},{6,8},{8,10},{10,12},{12,14},{14,16},{16,18},{18... | collective-permute-start | bytes 49160 | tf_op jit(solution)/shard_map/ppermute | solution.py:10
  10.9 0.8 dynamic_slice.10
  11.6 1.3 collective-permute-done
  12.9 1.0 maximum_convert_fusion
  14.0 2.1 fusion.37
  16.1 0.3 fusion.38
  16.4 0.1 fusion.34
  16.5 2.1 fusion.9
  18.7 0.1 copy.32
  18.8 0.1 eq.44
  18.9 0.1 eq.40
  19.0 1.2 reduce-window.6
  20.2 0.2 slice_reduce_fusion
  20.6 0.1 reduce_sum.41
  20.8 0.4 fusion.11
  21.1 8.9 %reduce-scatter.3.cloned.1.call-done = f32[128,2048]{1,0:T(8,128)} async-done(((f32[256,2048]{1,0:T(8,128)}), f32[128,2048]{1,0:T(8,128)}) %reduce-scatter.3.cloned.1.call-update) | async-done | bytes 1048592 | tf_op jit(solution)/shard_map/reduce_scatter | solution.py:66
  30.0 1.5 fusion.12
  31.5 1.3 convolution_convert_fusion.1
  32.8 98.8 %all_to_all.10 = bf16[16,64,2048]{2,1,0:T(8,128)(2,1)} all-to-all(bf16[16,64,2048]{2,1,0:T(8,128)(2,1)S(1)} %bitcast.45), channel_id=1, replica_groups=mesh['sp'=16,'tp'=2] {'sp'}, dimensions={0} | all-to-all | bytes 8388608 | tf_op jit(solution)/shard_map/all_to_all | solution.py:104
  131.7 0.2 reduce-scatter.5.cloned.1.call-start
  131.9 20.0 %all-gather.2.cloned.1.call-done = bf16[32,64,2048]{2,1,0:T(8,128)(2,1)} async-done(((bf16[16,64,2048]{2,1,0:T(8,128)(2,1)}), bf16[32,64,2048]{2,1,0:T(8,128)(2,1)}) %all-gather.2.cloned.1.call-update) | async-done | bytes 8388624 | tf_op jit(solution)/shard_map/all_gather | solution.py:103
  151.9 14.4 %fusion.1 = f32[2048,1024]{1,0:T(8,128)} fusion(bf16[2048,2048]{1,0:T(8,128)(2,1)} %bitcast.50, bf16[1,2048,1024]{2,1,0:T(8,128)(2,1)} %param.19), kind=kOutput, calls=%fused_computation.4 | convolution fusion | flops 8589934592 | bytes 20971520 | tf_op jit(solution)/shard_map/dot_general | solution.py:14
  166.4 26.9 %convolution_convert_fusion = bf16[2048,2048]{1,0:T(8,128)(2,1)} fusion(f32[2048,1024]{1,0:T(8,128)} %fusion.1, bf16[2048,2048]{1,0:T(8,128)(2,1)} %bitcast.51, bf16[1,1024,2048]{2,1,0:T(8,128)(2,1)} %param.21, bf16[1,2048,1024]{2,1,0:T(8,128)(2,1)} %param.20), kind=kOutput, calls=%fused_computation.2 | convolution fusion | flops 17205035008 | bytes 33554432 | tf_op jit(solution)/shard_map/dot_general | solution.py:21
  193.3 17.9 %reduce-scatter.5.cloned.1.call-done = bf16[16,64,2048]{2,1,0:T(8,128)(2,1)} async-done(((bf16[32,64,2048]{2,1,0:T(8,128)(2,1)}), bf16[16,64,2048]{2,1,0:T(8,128)(2,1)}) %reduce-scatter.5.cloned.1.call-update) | async-done | bytes 4194320 | tf_op jit(solution)/shard_map/reduce_scatter | solution.py:113
  211.1 7.0 %all-to-all-start.1 = ((bf16[16,64,2048]{2,1,0:T(8,128)(2,1)}), bf16[16,64,2048]{2,1,0:T(8,128)(2,1)}, u32[]{:S(2)}, u32[]{:S(2)}) async-start(bf16[16,64,2048]{2,1,0:T(8,128)(2,1)} %reduce-scatter.5.cloned.1.call-done), calls=%async_computation.3 | async-start | bytes 8388608 | tf_op jit(solution)/shard_map/all_to_all | solution.py:117
  218.2 0.1 copy.37
  218.4 95.2 %all-to-all-done.1 = bf16[16,64,2048]{2,1,0:T(8,128)(2,1)} async-done(((bf16[16,64,2048]{2,1,0:T(8,128)(2,1)}), bf16[16,64,2048]{2,1,0:T(8,128)(2,1)}, u32[]{:S(2)}, u32[]{:S(2)}) %all-to-all-start.1) | async-done | bytes 4194336 | tf_op jit(solution)/shard_map/all_to_all | solution.py:117
  313.6 7.1 %gather_fusion = bf16[512,2048]{1,0:T(8,128)(2,1)S(1)} fusion(bf16[1024,2048]{1,0:T(8,128)(2,1)} %bitcast.9, s32[1024]{0:T(1024)S(1)} %pad_clamp_fusion), kind=kCustom, calls=%fused_computation | custom fusion | bytes 4196352 | tf_op jit(solution)/shard_map/gather | solution.py:120
  320.8 3.0 reshape.194
  323.8 5.4 %multiply_reduce_fusion = f32[128,2048]{1,0:T(8,128)S(1)} fusion(f32[128,4,2048]{2,1,0:T(4,128)} %reshape.194, f32[128,4]{1,0:T(8,128)S(1)} %copy.37), kind=kLoop, calls=%fused_computation.7 | loop fusion | flops 1835008 | bytes 5244928 | tf_op jit(solution)/shard_map/reduce_sum | solution.py:122
  329.2 0.9 fusion.15
  (42 shorter events, 0.6 us)
Async XLA Ops:
  6.5 9.5 %copy-start = (bf16[4,256,256]{2,1,0:T(8,128)(2,1)S(1)}, bf16[4,256,256]{2,1,0:T(8,128)(2,1)}, u32[]{:S(2)}) copy-start(bf16[4,256,256]{2,1,0:T(8,128)(2,1)} %param.13) | copy-start | bytes 1572868
  6.5 23.5 %reduce-scatter.3.cloned.1.call-start = ((), (), s32[]{:S(2)}) async-start(), calls=%async_computation.4 | async-start | bytes 3145728 | tf_op jit(solution)/shard_map/reduce_scatter | solution.py:66
  7.3 5.6 %collective-permute-start = (bf16[16,512]{1,0:T(8,128)(2,1)S(1)}, bf16[16,512]{1,0:T(8,128)(2,1)S(1)}, u32[]{:S(2)}, u32[]{:S(2)}) collective-permute-start(bf16[16,512]{1,0:T(8,128)(2,1)S(1)} %slice.57), channel_id=1, source_target_pairs={{0,2},{2,4},{4,6},{6,8},{8,10},{10,12},{12,14},{14,16},{16,18},{18... | collective-permute-start | bytes 49160 | tf_op jit(solution)/shard_map/ppermute | solution.py:10
  13.9 2.6 copy-start.2
  16.1 2.6 copy-start.6
  16.4 13.7 %copy-start.3 = (bf16[128,2048]{1,0:T(8,128)(2,1)S(1)}, bf16[128,2048]{1,0:T(8,128)(2,1)}, u32[]{:S(2)}) copy-start(bf16[128,2048]{1,0:T(8,128)(2,1)} %param.12) | copy-start | bytes 1572868
  16.5 15.0 %copy-start.5 = (f32[2048]{0:T(1024)S(1)}, f32[2048]{0:T(1024)}, u32[]{:S(2)}) copy-start(f32[2048]{0:T(1024)} %param.16) | copy-start | bytes 24580
  18.6 133.3 %all-gather.2.cloned.1.call-start = ((), (), s32[]{:S(2)}) async-start(), calls=%async_computation.5 | async-start | bytes 12582912 | tf_op jit(solution)/shard_map/all_gather | solution.py:103
  131.7 79.4 %reduce-scatter.5.cloned.1.call-start = ((), (), s32[]{:S(2)}) async-start(), calls=%async_computation.6 | async-start | bytes 12582912 | tf_op jit(solution)/shard_map/reduce_scatter | solution.py:113
  193.2 24.9 %copy-start.4 = (f32[128,4]{0,1:T(4,128)S(1)}, f32[128,4]{0,1:T(4,128)}, u32[]{:S(2)}) copy-start(f32[128,4]{0,1:T(4,128)} %param.18) | copy-start | bytes 6148
  211.1 102.5 %all-to-all-start.1 = ((bf16[16,64,2048]{2,1,0:T(8,128)(2,1)}), bf16[16,64,2048]{2,1,0:T(8,128)(2,1)}, u32[]{:S(2)}, u32[]{:S(2)}) async-start(bf16[16,64,2048]{2,1,0:T(8,128)(2,1)} %reduce-scatter.5.cloned.1.call-done), calls=%async_computation.3 | async-start | bytes 8388608 | tf_op jit(solution)/shard_map/all_to_all | solution.py:117
  320.7 9.4 %copy-start.1 = (bf16[4,256,256]{2,1,0:T(8,128)(2,1)S(1)}, bf16[4,256,256]{2,1,0:T(8,128)(2,1)}, u32[]{:S(2)}) copy-start(bf16[4,256,256]{2,1,0:T(8,128)(2,1)} %param.13) | copy-start | bytes 1572868
Sparse Core Ops, SparseCore 0:
  18.8 11.2 reduce-scatter.2
  131.8 20.0 all-gather.1
  193.4 17.7 reduce-scatter.4
where the time goes:
time: 337 us
  waiting for transfers between devices  143 us (42%)
  blocking collectives  98.8 us (29%)
  matrix products  45 us (13%)
  between operations  13.4 us (4%)
  other arithmetic  12.9 us (4%)
  local copies, waits for them, and re-layouts  12.7 us (4%)
  starting transfers between devices  10.6 us (3%)
    all_to_all x1, blocking collectives, shards(): lax.all_to_all(outgoing, 'sp', split_axis=0, concat_axis=0, tiled=True)  98.8 us
    all_to_all x1, waiting for transfers between devices, shards(): lax.all_to_all(summed, 'sp', split_axis=0, concat_axis=0, tiled=True)  95.2 us
    dot_general x1, matrix products, expert_half(): jnp.dot(activated, down_local, preferred_element_type=jnp.float32)  26.9 us
    all_gather x1, waiting for transfers between devices, shards(): lax.all_gather(lax.all_to_all(outgoing, 'sp', split_axis=0, concat_axis=0...  20 us
    reduce_scatter x1, waiting for transfers between devices, shards(): lax.psum_scatter(partial_value, 'tp', scatter_dimension=0, tiled=True)  17.9 us
    dot_general x1, matrix products, expert_half(): gate_pre = jnp.dot(rows, gate_local, preferred_element_type=jnp.float32)  14.4 us
    reduce_scatter x1, waiting for transfers between devices, shards(): lax.psum_scatter(jnp.dot(mixer_out, own_rows, preferred_element_type=jnp....  8.87 us
    gather x1, local copies, waits for them, and re-layouts, shards(): expert_flat[slot_ids].astype(jnp.float32)  7.13 us
  transfers between devices with their start and end apart: 5, of which 5 were waited for; matrix products, arithmetic and copies ran while one was open for 1% of the time, Pallas kernels for 0%

commit v1 on v0

v1 whole, which is shorter than its diff:
```python
import functools

import jax
import jax.numpy as jnp
from jax import lax
from jax.experimental import pallas as pl
from jax.experimental.pallas import tpu as pltpu
from jax.sharding import PartitionSpec as P

MESH = pl.DeviceIdType.MESH
F32, BF16 = jnp.float32, jnp.bfloat16


def xor(index, mask):
    out, bit = index, 1
    while bit <= mask:
        if mask // bit % 2:
            out = out + bit - 2 * bit * (index // bit % 2)
        bit *= 2
    return out


def layer_kernel(
    planes,
    ways,
    cap,
    normed_ref,
    meta_ref,
    middle_ref,
    gate_hbm,
    up_hbm,
    down_hbm,
    out_ref,
    gate_w,
    up_w,
    down_w,
    tok,
    metas,
    snd,
    rows,
    act,
    part,
    part_in,
    back,
    mix_in,
    acc,
    w_sem,
    z_sem,
    m_sem,
    a_send,
    a_recv,
    f_sem,
    p_sem,
    r_send,
    r_recv,
    x_sem,
):
    sp, core = lax.axis_index("sp"), lax.axis_index("tp")
    z, p = sp // ways, sp % ways
    tokens, width = normed_ref.shape
    hidden = gate_w.shape[1]
    experts = meta_ref.shape[0] // 2

    def z_peer(k):
        return (xor(z, k) * ways + p, core)

    def p_peer(q):
        return (z * ways + xor(p, q), core)

    sibling = (sp, 1 - core)

    barrier = pltpu.get_barrier_semaphore()
    for k in range(1, planes):
        pl.semaphore_signal(barrier, inc=1, device_id=z_peer(k), device_id_type=MESH)
    for q in range(1, ways):
        pl.semaphore_signal(barrier, inc=1, device_id=p_peer(q), device_id_type=MESH)
    pl.semaphore_signal(barrier, inc=1, device_id=sibling, device_id_type=MESH)
    pl.semaphore_wait(barrier, planes + ways - 1)

    def remote(src, dst, send, recv, device):
        return pltpu.make_async_remote_copy(
            src_ref=src,
            dst_ref=dst,
            send_sem=send,
            recv_sem=recv,
            device_id=device,
            device_id_type=MESH,
        )

    z_copies, m_copies = {}, {}
    for k in range(1, planes):
        m_copies[k] = remote(meta_ref, metas.at[k], m_sem.at[0, k], m_sem.at[1, k], z_peer(k))
        m_copies[k].start()
    for k in range(1, planes):
        z_copies[k] = remote(normed_ref, tok.at[k], z_sem.at[0, k], z_sem.at[1, k], z_peer(k))
        z_copies[k].start()
    loads = [
        pltpu.make_async_copy(src, dst, w_sem.at[i])
        for i, (src, dst) in enumerate(((gate_hbm, gate_w), (up_hbm, up_w), (down_hbm, down_w)))
    ]
    for load in loads:
        load.start()

    slot_of = lax.broadcasted_iota(jnp.int32, (cap, tokens), 0).astype(F32)

    def meta_row(k, row):
        if k == 0:
            return meta_ref[pl.ds(row, 1), :]
        return metas[k, pl.ds(row, 1), :]

    a_copies, r_copies, f_copies, p_copies, x_copies = {}, {}, {}, {}, {}

    def pick(k):
        if k:
            m_copies[k].wait_recv()
            z_copies[k].wait_recv()
        source = normed_ref if k == 0 else tok.at[k]
        order = list(range(1, ways)) + [0]
        for q in order:
            expert = z * ways + xor(p, q)
            choose = jnp.where(meta_row(k, expert) == slot_of, 1.0, 0.0).astype(BF16)
            chosen = jnp.dot(choose, source[...], preferred_element_type=F32).astype(BF16)
            if q == 0:
                rows[k, core, 0] = chosen
            else:
                snd[k, q] = chosen
                a_copies[k, q] = remote(
                    snd.at[k, q], rows.at[k, core, q], a_send.at[k, q], a_recv.at[k, q], p_peer(q)
                )
                a_copies[k, q].start()

    def forward(k):
        for q in range(1, ways):
            a_copies[k, q].wait_recv()
        f_copies[k] = remote(
            rows.at[k, core], rows.at[k, core], f_sem.at[0, k], f_sem.at[1, k], sibling
        )
        f_copies[k].start()

    half = ways * cap
    step_f = min(hidden, 256)
    step_d = min(width, 256)

    def expert(k):
        f_copies[k].wait_recv()

        def gated(i, carry):
            cols = pl.ds(pl.multiple_of(i * step_f, step_f), step_f)
            these = rows[k].reshape(2 * half, width)
            gate_pre = jnp.dot(these, gate_w[:, cols], preferred_element_type=F32)
            up_pre = jnp.dot(these, up_w[:, cols], preferred_element_type=F32)
            a = jnp.minimum(gate_pre, 7.0)
            b = jnp.clip(up_pre, -7.0, 7.0) + 1.0
            act[:, cols] = (b * (a * jax.nn.sigmoid(1.702 * a))).astype(BF16)
            return carry

        lax.fori_loop(0, hidden // step_f, gated, 0)

        def down(i, carry):
            cols = pl.ds(pl.multiple_of(i * step_d, step_d), step_d)
            value = jnp.dot(act[...], down_w[:, cols], preferred_element_type=F32).astype(BF16)
            part[k, :, :, cols] = value.reshape(2, half, step_d)
            return carry

        if k == 0:
            loads[2].wait()
        lax.fori_loop(0, width // step_d, down, 0)
        p_copies[k] = remote(
            part.at[k, 1 - core], part_in.at[k], p_sem.at[0, k], p_sem.at[1, k], sibling
        )
        p_copies[k].start()

    def give_back(k):
        p_copies[k].wait_recv()
        for q in list(range(1, ways)) + [0]:
            here = pl.ds(q * cap, cap)
            total = (part[k, core, here, :].astype(F32) + part_in[k, here, :].astype(F32)).astype(
                BF16
            )
            if q == 0:
                back[k, 0] = total
            else:
                a_copies[k, q].wait_send()
                snd[k, q] = total
                r_copies[k, q] = remote(
                    snd.at[k, q], back.at[k, q], r_send.at[k, q], r_recv.at[k, q], p_peer(q)
                )
                r_copies[k, q].start()

    def combine(k):
        blocks = []
        for q in range(ways):
            if q:
                r_copies[k, q].wait_recv()
            index = z * ways + xor(p, q)
            blocks.append(
                jnp.where(meta_row(k, index) == slot_of, meta_row(k, index + experts), 0.0)
            )
        mixer = jnp.transpose(jnp.concatenate(blocks, axis=0))
        high = mixer.astype(BF16)
        low = (mixer - high.astype(F32)).astype(BF16)

        def mixed(i, carry):
            cols = pl.ds(pl.multiple_of(i * step_d, step_d), step_d)
            values = back[k, :, :, cols].reshape(half, step_d)
            total = jnp.dot(high, values, preferred_element_type=F32) + jnp.dot(
                low, values, preferred_element_type=F32
            )
            if k == 0:
                acc[:, cols] = total
            else:
                tok[k, :, cols] = total.astype(BF16)
            return carry

        lax.fori_loop(0, width // step_d, mixed, 0)
        if k:
            x_copies[k] = remote(
                tok.at[k], mix_in.at[k], x_sem.at[0, k], x_sem.at[1, k], z_peer(k)
            )
            x_copies[k].start()

    pick(0)
    loads[0].wait()
    loads[1].wait()
    for k in range(planes):
        if k + 1 < planes:
            forward(k)
            pick(k + 1)
        else:
            forward(k)
        expert(k)
        if k:
            combine(k - 1)
        give_back(k)
    combine(planes - 1)

    for k in range(1, planes):
        x_copies[k].wait_recv()
        acc[...] += mix_in[k].astype(F32)
    out_ref[...] = (middle_ref[...].astype(F32) + acc[...]).astype(out_ref.dtype)

    for k in range(1, planes):
        m_copies[k].wait_send()
        z_copies[k].wait_send()
        x_copies[k].wait_send()
    for k in range(planes):
        f_copies[k].wait_send()
        p_copies[k].wait_send()
        for q in range(1, ways):
            r_copies[k, q].wait_send()


def experts_layer(normed, meta, middle, gate, up, down, cap):
    tokens, width = normed.shape
    hidden = gate.shape[1]
    size = lax.axis_size("sp")
    planes = 1 << ((size.bit_length() - 1) // 2)
    ways = size // planes
    vmem = pl.BlockSpec(memory_space=pltpu.VMEM)
    hbm = pl.BlockSpec(memory_space=pltpu.HBM)
    dma = pltpu.SemaphoreType.DMA
    return pl.pallas_call(
        functools.partial(layer_kernel, planes, ways, cap),
        out_shape=jax.ShapeDtypeStruct((tokens, width), BF16),
        in_specs=[vmem, vmem, vmem, hbm, hbm, hbm],
        out_specs=vmem,
        scratch_shapes=[
            pltpu.VMEM((width, hidden), BF16),
            pltpu.VMEM((width, hidden), BF16),
            pltpu.VMEM((hidden, width), BF16),
            pltpu.VMEM((planes, tokens, width), BF16),
            pltpu.VMEM((planes,) + meta.shape, F32),
            pltpu.VMEM((planes, ways, cap, width), BF16),
            pltpu.VMEM((planes, 2, ways, cap, width), BF16),
            pltpu.VMEM((2 * ways * cap, hidden), BF16),
            pltpu.VMEM((planes, 2, ways * cap, width), BF16),
            pltpu.VMEM((planes, ways * cap, width), BF16),
            pltpu.VMEM((planes, ways, cap, width), BF16),
            pltpu.VMEM((planes, tokens, width), BF16),
            pltpu.VMEM((tokens, width), F32),
            dma((3,)),
            dma((2, planes)),
            dma((2, planes)),
            dma((planes, ways)),
            dma((planes, ways)),
            dma((2, planes)),
            dma((2, planes)),
            dma((planes, ways)),
            dma((planes, ways)),
            dma((2, planes)),
        ],
        compiler_params=pltpu.CompilerParams(
            collective_id=0, has_side_effects=True, vmem_limit_bytes=67043328 - (2 << 20)
        ),
    )(normed, meta, middle, gate, up, down)


def shards(
    pool_input,
    residual,
    pool_weight,
    pool_gain,
    out_weight,
    norm_gain,
    routes,
    route_scores,
    gate_weight,
    up_weight,
    down_weight,
):
    tokens_here, width_here = pool_input.shape
    cores = lax.axis_size("tp")
    groups, group_dim = pool_weight.shape[:2]
    core = lax.axis_index("tp")
    count = tokens_here // cores
    reach = 1 << groups
    devices = lax.axis_size("sp")
    previous = lax.ppermute(
        pool_input[tokens_here - reach :], "sp", [(i, i + 1) for i in range(devices - 1)]
    )
    extended = jnp.concatenate([previous, pool_input], axis=0)
    theirs = lax.ppermute(
        lax.dynamic_slice_in_dim(extended, (1 - core) * count, count + reach, 0),
        "tp",
        [(0, 1), (1, 0)],
    )
    mine = lax.dynamic_slice_in_dim(extended, core * count, count + reach, 0)
    first = core == 0
    halves = (jnp.where(first, mine, theirs), jnp.where(first, theirs, mine))
    values = jnp.concatenate(halves, axis=1).astype(F32)
    positions = (
        lax.axis_index("sp") * tokens_here + core * count + jnp.arange(count)
    ).astype(F32)[:, None]
    pieces = []
    for group in range(groups):
        total = values[:, group * group_dim : (group + 1) * group_dim]
        here = total[reach:]
        for level in range(group + 1):
            shift = 1 << level
            total = total[shift:] + total[:-shift]
        window = 2 << group
        total = total[total.shape[0] - count :]
        pooled = (total / jnp.minimum(positions + 1.0, float(window)) - here).astype(BF16)
        pieces.append(jnp.dot(pooled, pool_weight[group], preferred_element_type=F32))
    mixer_out = (jnp.concatenate(pieces, axis=1) * pool_gain[None, :]).astype(BF16)
    projected = jnp.dot(mixer_out, out_weight, preferred_element_type=F32)
    middle = (residual.astype(F32) + projected).astype(BF16)
    wide = middle.astype(F32)
    normed = (
        wide
        * lax.rsqrt(jnp.mean(wide * wide, axis=1, keepdims=True) + 1e-05)
        * norm_gain[None, :]
    ).astype(BF16)
    weights = jax.nn.softmax(route_scores, axis=-1)
    row_count, top_count = routes.shape
    experts_total = gate_weight.shape[0] * devices
    cap = row_count * top_count * cores // experts_total
    named = routes.T[:, None, :] == jnp.arange(experts_total)[None, :, None]
    hits = jnp.any(named, axis=0)
    share = jnp.sum(jnp.where(named, weights.T[:, None, :], 0.0), axis=0)
    before = (jnp.arange(row_count)[:, None] < jnp.arange(row_count)[None, :]).astype(BF16)
    rank = jnp.dot(hits.astype(BF16), before, preferred_element_type=F32)
    meta = jnp.concatenate([jnp.where(hits, rank, -1.0), share], axis=0)
    return experts_layer(
        normed, meta, middle, gate_weight[0], up_weight[0], down_weight[0], cap
    )


def solution(mesh):
    return jax.shard_map(
        shards,
        mesh=mesh,
        in_specs=(
            P("sp", "tp"),
            P(("sp", "tp"), None),
            P(),
            P(),
            P(),
            P(),
            P(("sp", "tp"), None),
            P(("sp", "tp"), None),
            P("sp", None, "tp"),
            P("sp", None, "tp"),
            P("sp", "tp", None),
        ),
        out_specs=P(("sp", "tp"), None),
        check_vma=False,
    )
```

time: 337 us -> 158 us (0.47)
  waiting for transfers between devices: 143 us -> 0.74 us
  Pallas kernels: 0 us -> 140 us
  blocking collectives: 98.8 us -> 0 us
  matrix products: 45 us -> 1.91 us
  between operations: 13.4 us -> 0.21 us
  local copies, waits for them, and re-layouts: 12.7 us -> 4.9 us
  other arithmetic: 12.9 us -> 5.33 us
  starting transfers between devices: 10.6 us -> 3.46 us
    pallas_call x0 -> x1, Pallas kernels: none -> 140 us  [experts_layer(): pl.pallas_call(functools.partial(layer_kernel, planes, ways, cap), out_sh...]
    all_to_all x1 -> x0, blocking collectives: 98.8 us -> none  [shards(): lax.all_to_all(outgoing, 'sp', split_axis=0, concat_axis=0, tiled=True)]
    all_to_all x1 -> x0, waiting for transfers between devices: 95.2 us -> none  [shards(): lax.all_to_all(summed, 'sp', split_axis=0, concat_axis=0, tiled=True)]
    dot_general x5 -> x6, matrix products: 45 us -> 1.91 us  [the longest x1 0.92 us: shards(): projected = jnp.dot(mixer_out, out_weight, preferred_element_type=F32)]
    reduce_scatter x2 -> x0, waiting for transfers between devices: 26.7 us -> none  [the longest x1 17.9 us: shards(): lax.psum_scatter(partial_value, 'tp', scatter_dimension=0, tiled=True)]
    all_gather x1 -> x0, waiting for transfers between devices: 20 us -> none  [shards(): lax.all_gather(lax.all_to_all(outgoing, 'sp', split_axis=0, concat_axis=0...]
    gather x1 -> x0, local copies, waits for them, and re-layouts: 7.13 us -> none  [shards(): expert_flat[slot_ids].astype(jnp.float32)]
    all_to_all x1 -> x0, starting transfers between devices: 6.96 us -> none  [shards(): lax.all_to_all(summed, 'sp', split_axis=0, concat_axis=0, tiled=True)]
  transfers between devices with their start and end apart: 5 -> 2, of which waited for: 5 -> 1; matrix products, arithmetic and copies ran while one was open for 1% -> 3% of each run, Pallas kernels for 0% -> 0%
where the time goes in v1:
time: 158 us; the launch traced here: 157 us
  Pallas kernels  140 us (89%)
  other arithmetic  5.33 us (3%)
  local copies, waits for them, and re-layouts  4.9 us (3%)
  starting transfers between devices  3.46 us (2%)
  matrix products  1.91 us (1%)
    pallas_call x1, Pallas kernels, experts_layer(): pl.pallas_call(functools.partial(layer_kernel, planes, ways, cap), out_sh...  140 us
    ppermute x1, starting transfers between devices, shards(): lax.ppermute(pool_input[tokens_here - reach:], 'sp', [(i, i + 1) for i in...  3.39 us
  transfers between devices with their start and end apart: 2, of which 1 were waited for; matrix products, arithmetic and copies ran while one was open for 3% of the time, Pallas kernels for 0%

profile of v1, /device:TPU:14, one launch (start us, length us, event | category | flops | bytes accessed | tf_op | source)
XLA Modules:
  0.0 156.6 jit_solution(6030183958241101259)
XLA Ops:
  0.0 0.8 slice.115
  0.8 3.4 %collective-permute-start = (bf16[16,512]{1,0:T(8,128)(2,1)S(1)}, bf16[16,512]{1,0:T(8,128)(2,1)S(1)}, u32[]{:S(2)}, u32[]{:S(2)}) collective-permute-start(bf16[16,512]{1,0:T(8,128)(2,1)S(1)} %slice.115), channel_id=1, source_target_pairs={{0,2},{2,4},{4,6},{6,8},{8,10},{10,12},{12,14},{14,16},{16,18},{18... | collective-permute-start | bytes 49160 | tf_op jit(solution)/shard_map/ppermute | solution.py:318
  4.2 0.7 reduce_max.9
  4.9 0.7 fusion.32
  5.6 0.7 divide_bitcast_fusion
  6.3 0.7 fusion.31
  7.0 0.1 convolution_select_fusion
  7.1 0.7 select_reduce_fusion
  7.8 0.0 collective-permute-done
  7.8 1.0 constant_dynamic-update-slice_fusion
  8.8 0.1 collective-permute-start.1
  8.9 0.6 pad_maximum_fusion.meta_ref
  9.5 0.7 collective-permute-done.1
  10.3 0.1 broadcast_select_fusion.1
  10.3 0.1 maximum_convert_fusion
  10.4 0.0 copy-start.2
  10.4 0.0 copy-start.4
  10.4 0.0 copy-start.5
  10.4 0.1 fusion.34
  10.7 0.0 copy-done.3
  10.7 0.2 fusion.21
  10.9 0.0 copy-start.1
  10.9 0.2 fusion.15
  11.1 0.2 fusion.17
  11.3 0.2 fusion.19
  11.6 1.0 copy-done.2
  12.6 0.1 copy-done.4
  12.7 0.9 fusion.1
  13.7 1.0 fusion.3.normed_ref
  14.7 0.0 copy-done
  14.7 140.0 %shard_map.109 = bf16[128,2048]{1,0:T(8,128)(2,1)} custom-call(bf16[128,2048]{1,0:T(8,128)(2,1)} %fusion.3.normed_ref, f32[32,128]{1,0:T(8,128)} %pad_maximum_fusion.meta_ref, bf16[128,2048]{1,0:T(8,128)(2,1)} %copy-done, bf16[2048,1024]{1,0:T(8,128)(2,1)} %bitcast.20, bf16[2048,1024]{1,0:T(8,128)(2,1)} %bitcast.21, bf16[1024,2048]{1,0:T(8,128)(2,1)} %bitcast.22), custom_call_target="tpu_custom_call" | custom-call | tf_op jit(solution)/shard_map/pallas_call | solution.py:262
  154.7 1.9 %copy.14 = bf16[128,2048]{1,0:T(8,128)(2,1)} copy(bf16[128,2048]{1,0:T(8,128)(2,1)} %shard_map.109) | data formatting | bytes 1048576
  (14 shorter events, 0.2 us)
Async XLA Ops:
  0.0 10.7 %copy-start.3 = (bf16[4,256,256]{2,1,0:T(8,128)(2,1)S(1)}, bf16[4,256,256]{2,1,0:T(8,128)(2,1)}, u32[]{:S(2)}) copy-start(bf16[4,256,256]{2,1,0:T(8,128)(2,1)} %param.13) | copy-start | bytes 1572868
  0.8 7.0 %collective-permute-start = (bf16[16,512]{1,0:T(8,128)(2,1)S(1)}, bf16[16,512]{1,0:T(8,128)(2,1)S(1)}, u32[]{:S(2)}, u32[]{:S(2)}) collective-permute-start(bf16[16,512]{1,0:T(8,128)(2,1)S(1)} %slice.115), channel_id=1, source_target_pairs={{0,2},{2,4},{4,6},{6,8},{8,10},{10,12},{12,14},{14,16},{16,18},{18... | collective-permute-start | bytes 49160 | tf_op jit(solution)/shard_map/ppermute | solution.py:318
  8.8 1.4 collective-permute-start.1
  10.4 2.2 %copy-start.2 = (bf16[1024,2048]{1,0:T(8,128)(2,1)S(1)}, bf16[1024,2048]{1,0:T(8,128)(2,1)}, u32[]{:S(2)}) copy-start(bf16[1024,2048]{1,0:T(8,128)(2,1)} %param.15) | copy-start | bytes 12582916
  10.4 2.3 %copy-start.4 = (bf16[128,2048]{1,0:T(8,128)(2,1)S(1)}, bf16[128,2048]{1,0:T(8,128)(2,1)}, u32[]{:S(2)}) copy-start(bf16[128,2048]{1,0:T(8,128)(2,1)} %param.12) | copy-start | bytes 1572868
  10.4 2.3 %copy-start.5 = (f32[1024]{0:T(1024)S(1)}, f32[1024]{0:T(1024)}, u32[]{:S(2)}) copy-start(f32[1024]{0:T(1024)} %param.14) | copy-start | bytes 12292
  10.9 2.8 %copy-start.1 = (f32[2048]{0:T(1024)S(1)}, f32[2048]{0:T(1024)}, u32[]{:S(2)}) copy-start(f32[2048]{0:T(1024)} %param.16) | copy-start | bytes 24580
  13.6 1.0 copy-start

commit v2 on v1

--- a/solution.py
+++ b/solution.py
@@ -91,9 +91,16 @@
     for k in range(1, planes):
         m_copies[k] = remote(meta_ref, metas.at[k], m_sem.at[0, k], m_sem.at[1, k], z_peer(k))
         m_copies[k].start()
-    for k in range(1, planes):
+    order = [0] + list(range(planes - 1, 0, -1))
+    relayed = planes >= 4
+
+    def send_own(k):
         z_copies[k] = remote(normed_ref, tok.at[k], z_sem.at[0, k], z_sem.at[1, k], z_peer(k))
         z_copies[k].start()
+
+    for k in order[1:]:
+        if not relayed or k > 2:
+            send_own(k)
     loads = [
         pltpu.make_async_copy(src, dst, w_sem.at[i])
         for i, (src, dst) in enumerate(((gate_hbm, gate_w), (up_hbm, up_w), (down_hbm, down_w)))
@@ -114,9 +121,12 @@
         if k:
             m_copies[k].wait_recv()
             z_copies[k].wait_recv()
+        if relayed and k == 3:
+            z_copies[2] = remote(tok.at[3], tok.at[2], z_sem.at[0, 2], z_sem.at[1, 2], z_peer(1))
+            z_copies[2].start()
+            send_own(1)
         source = normed_ref if k == 0 else tok.at[k]
-        order = list(range(1, ways)) + [0]
-        for q in order:
+        for q in list(range(1, ways)) + [0]:
             expert = z * ways + xor(p, q)
             choose = jnp.where(meta_row(k, expert) == slot_of, 1.0, 0.0).astype(BF16)
             chosen = jnp.dot(choose, source[...], preferred_element_type=F32).astype(BF16)
@@ -188,6 +198,8 @@
                 r_copies[k, q].start()
 
     def combine(k):
+        if relayed and k == 3:
+            z_copies[2].wait_send()
         blocks = []
         for q in range(ways):
             if q:
@@ -222,17 +234,15 @@
     pick(0)
     loads[0].wait()
     loads[1].wait()
-    for k in range(planes):
-        if k + 1 < planes:
-            forward(k)
-            pick(k + 1)
-        else:
-            forward(k)
+    for i, k in enumerate(order):
+        forward(k)
+        if i + 1 < planes:
+            pick(order[i + 1])
         expert(k)
-        if k:
-            combine(k - 1)
+        if i:
+            combine(order[i - 1])
         give_back(k)
-    combine(planes - 1)
+    combine(order[-1])
 
     for k in range(1, planes):
         x_copies[k].wait_recv()
@@ -241,7 +251,8 @@
 
     for k in range(1, planes):
         m_copies[k].wait_send()
-        z_copies[k].wait_send()
+        if not relayed or k != 2:
+            z_copies[k].wait_send()
         x_copies[k].wait_send()
     for k in range(planes):
         f_copies[k].wait_send()

time: 158 us -> 152 us (0.962)
  the two profiles are of different devices: /device:TPU:14 before, /device:TPU:0 now
where the time goes in v2:
time: 152 us
  Pallas kernels  134 us (88%)
  other arithmetic  5.33 us (4%)
  starting transfers between devices  4.93 us (3%)
  local copies, waits for them, and re-layouts  4.9 us (3%)
  matrix products  1.91 us (1%)
    pallas_call x1, Pallas kernels, experts_layer(): pl.pallas_call(functools.partial(layer_kernel, planes, ways, cap), out_sh...  134 us
    ppermute x1, starting transfers between devices, shards(): lax.ppermute(pool_input[tokens_here - reach:], 'sp', [(i, i + 1) for i in...  4.86 us
    unnamed x14, local copies, waits for them, and re-layouts  3.07 us
  transfers between devices with their start and end apart: 2, of which 1 were waited for; matrix products, arithmetic and copies ran while one was open for 3% of the time, Pallas kernels for 0%

profile of v2, /device:TPU:0, one launch (start us, length us, event | category | flops | bytes accessed | tf_op | source)
XLA Modules:
  0.0 152.1 jit_solution(5020470675726568652)
XLA Ops:
  0.0 0.8 slice.115
  0.8 4.9 %collective-permute-start = (bf16[16,512]{1,0:T(8,128)(2,1)S(1)}, bf16[16,512]{1,0:T(8,128)(2,1)S(1)}, u32[]{:S(2)}, u32[]{:S(2)}) collective-permute-start(bf16[16,512]{1,0:T(8,128)(2,1)S(1)} %slice.115), channel_id=1, source_target_pairs={{0,2},{2,4},{4,6},{6,8},{8,10},{10,12},{12,14},{14,16},{16,18},{18... | collective-permute-start | bytes 49160 | tf_op jit(solution)/shard_map/ppermute | solution.py:329
  5.7 0.7 reduce_max.9
  6.4 0.7 fusion.32
  7.1 0.7 divide_bitcast_fusion
  7.7 0.7 fusion.31
  8.4 0.1 convolution_select_fusion
  8.6 0.7 select_reduce_fusion
  9.3 0.0 collective-permute-done
  9.3 1.0 constant_dynamic-update-slice_fusion
  10.3 0.1 collective-permute-start.1
  10.4 0.6 pad_maximum_fusion.meta_ref
  11.0 0.7 collective-permute-done.1
  11.7 0.1 broadcast_select_fusion.1
  11.8 0.1 maximum_convert_fusion
  11.9 0.0 copy-start.2
  11.9 0.0 copy-start.4
  11.9 0.0 copy-start.5
  11.9 0.1 fusion.34
  12.1 0.0 copy-done.3
  12.2 0.2 fusion.21
  12.4 0.0 copy-start.1
  12.4 0.2 fusion.15
  12.6 0.2 fusion.17
  12.8 0.2 fusion.19
  13.0 1.0 copy-done.2
  14.1 0.1 copy-done.4
  14.2 0.9 fusion.1
  15.1 1.0 fusion.3.normed_ref
  16.1 0.0 copy-done
  16.1 134.1 %shard_map.109 = bf16[128,2048]{1,0:T(8,128)(2,1)} custom-call(bf16[128,2048]{1,0:T(8,128)(2,1)} %fusion.3.normed_ref, f32[32,128]{1,0:T(8,128)} %pad_maximum_fusion.meta_ref, bf16[128,2048]{1,0:T(8,128)(2,1)} %copy-done, bf16[2048,1024]{1,0:T(8,128)(2,1)} %bitcast.20, bf16[2048,1024]{1,0:T(8,128)(2,1)} %bitcast.21, bf16[1024,2048]{1,0:T(8,128)(2,1)} %bitcast.22), custom_call_target="tpu_custom_call" | custom-call | tf_op jit(solution)/shard_map/pallas_call | solution.py:273
  150.2 1.9 %copy.14 = bf16[128,2048]{1,0:T(8,128)(2,1)} copy(bf16[128,2048]{1,0:T(8,128)(2,1)} %shard_map.109) | data formatting | bytes 1048576
  (14 shorter events, 0.2 us)
Async XLA Ops:
  0.0 12.1 %copy-start.3 = (bf16[4,256,256]{2,1,0:T(8,128)(2,1)S(1)}, bf16[4,256,256]{2,1,0:T(8,128)(2,1)}, u32[]{:S(2)}) copy-start(bf16[4,256,256]{2,1,0:T(8,128)(2,1)} %param.13) | copy-start | bytes 1572868
  0.8 8.5 %collective-permute-start = (bf16[16,512]{1,0:T(8,128)(2,1)S(1)}, bf16[16,512]{1,0:T(8,128)(2,1)S(1)}, u32[]{:S(2)}, u32[]{:S(2)}) collective-permute-start(bf16[16,512]{1,0:T(8,128)(2,1)S(1)} %slice.115), channel_id=1, source_target_pairs={{0,2},{2,4},{4,6},{6,8},{8,10},{10,12},{12,14},{14,16},{16,18},{18... | collective-permute-start | bytes 49160 | tf_op jit(solution)/shard_map/ppermute | solution.py:329
  10.3 1.4 collective-permute-start.1
  11.9 2.2 %copy-start.2 = (bf16[1024,2048]{1,0:T(8,128)(2,1)S(1)}, bf16[1024,2048]{1,0:T(8,128)(2,1)}, u32[]{:S(2)}) copy-start(bf16[1024,2048]{1,0:T(8,128)(2,1)} %param.15) | copy-start | bytes 12582916
  11.9 2.3 %copy-start.4 = (bf16[128,2048]{1,0:T(8,128)(2,1)S(1)}, bf16[128,2048]{1,0:T(8,128)(2,1)}, u32[]{:S(2)}) copy-start(bf16[128,2048]{1,0:T(8,128)(2,1)} %param.12) | copy-start | bytes 1572868
  11.9 2.3 %copy-start.5 = (f32[1024]{0:T(1024)S(1)}, f32[1024]{0:T(1024)}, u32[]{:S(2)}) copy-start(f32[1024]{0:T(1024)} %param.14) | copy-start | bytes 12292
  12.4 2.8 %copy-start.1 = (f32[2048]{0:T(1024)S(1)}, f32[2048]{0:T(1024)}, u32[]{:S(2)}) copy-start(f32[2048]{0:T(1024)} %param.16) | copy-start | bytes 24580
  15.1 1.0 copy-start
